TPU v7x, 32 devices: a whole 2x2x4 slice. The times are simulated.
32 devices in a mesh: dp: 2 (over x), kv: 8 (over z, y), tp: 2 (over core).
Axes of the slice: x: 2, y: 2, z: 4, core: 2. Of those that a mesh axis runs over, the one named last changes fastest.
Arguments:
- tokens: bfloat16 [2, 1536, 2048], P('dp', 'kv'), may hold values from -60 to 60
- doc_lengths: int32 [2, 8], P('dp'), may hold values from 1 to 768, as said below
- picked: int32 [2, 48, 32], P('dp', 'kv'), may hold values from -1 to 47, as said below
- w_query: bfloat16 [2048, 1024], P(None, 'tp'), may hold values from -0.125 to 0.125
- w_key: bfloat16 [2048, 128], replicated, may hold values from -0.125 to 0.125
- w_value: bfloat16 [2048, 128], replicated, may hold values from -0.125 to 0.125
- w_out: bfloat16 [1024, 2048], replicated, may hold values from -0.1875 to 0.1875
Outputs:
- mixed: bfloat16 [2, 1536, 2048], P('dp', 'kv')
Inputs may be any that keep to these rules, and one draw needn't show every extreme that they name: `doc_lengths`: each row sums to 1536; its largest document has exactly 768 positions. `picked`: slot 0 of query block b is b itself; the other slots hold distinct blocks before b, or -1 when fewer such blocks are named. Of the 6 blocks that one device of kv holds, at most 2 are named by query blocks held by other devices of kv, and in every row some device reaches 2.
All inputs are finite; a program needn't handle non-finite values.
Results may differ from a plain program's by a relative error of at most 0.011.
Values may be sent and summed in bfloat16 or wider, within the bound.
A program may use at most 64 MiB of HBM per device.

v0:
```python
import functools
import math

import jax
import jax.numpy as jnp
import numpy as np
from jax import lax
from jax.experimental import pallas as pl
from jax.experimental.pallas import tpu as pltpu
from jax.sharding import PartitionSpec as P

HEAD_DIM = 64
BLOCK = 32
LANES = 128
HOT = 2
MESH = pl.DeviceIdType.MESH
SCALE = float(HEAD_DIM ** -0.5 * np.log2(np.e))
F32 = jnp.float32
BF16 = jnp.bfloat16


def tables(rows, count):
    lane = np.arange(LANES)
    half = HEAD_DIM // 2
    inverse = (10000.0 ** (-(lane % half) / half)).astype(np.float32).astype(np.float64)
    sign = np.where(lane % HEAD_DIM < half, -1.0, 1.0)
    row = np.arange(rows)[:, None] * inverse
    start = (np.arange(count) * rows)[:, None] * inverse
    inner = np.stack([np.cos(row), np.sin(row) * sign]).astype(np.float32)
    outer = np.zeros((count, 8, LANES), np.float32)
    outer[:, 0] = np.cos(start)
    outer[:, 1] = np.sin(start) * sign
    return inner, outer


def iota(shape, axis):
    return lax.broadcasted_iota(jnp.int32, shape, axis)


def dot_t(a, b):
    return lax.dot_general(a, b, (((1,), (1,)), ((), ())), preferred_element_type=F32)


def dot(a, b):
    return jnp.dot(a, b, preferred_element_type=F32)


def kernel(
    n, reach, tok_hbm, doc_hbm, pick_hbm, wq_hbm, wk_hbm, wv_hbm, wo_hbm, inner_hbm, outer_hbm, out,
    tok, doc, pick, wq, wkv, wo, inner, outer, names, names_in, kv_own, pack, hot_in, ids, ids_in,
    q_all, acc, top, att, att_in, partial, load_sem, name_s, name_r, hot_s, hot_r, ids_s, ids_r, att_s, att_r,
):
    kv = lax.axis_index("kv")
    tp = lax.axis_index("tp")
    rows = tok.shape[0]
    blocks = rows // BLOCK
    heads = wq.shape[1] // HEAD_DIM
    wide = names.shape[1]
    mine = wo.shape[1]

    barrier = pltpu.get_barrier_semaphore()

    before = jnp.minimum(kv, reach)
    after = jnp.minimum(n - 1 - kv, reach)

    def greet(d, _):
        @pl.when(d != kv)
        def _():
            pl.semaphore_signal(barrier, inc=1, device_id={"kv": d}, device_id_type=MESH)
        return 0

    lax.fori_loop(kv - before, kv + after + 1, greet, 0)
    pl.semaphore_signal(barrier, inc=1, device_id={"tp": 1 - tp}, device_id_type=MESH)

    pairs = [
        (pick_hbm, pick), (doc_hbm, doc), (tok_hbm.at[0], tok), (wk_hbm, wkv.at[:, 0:LANES]), (wv_hbm, wkv.at[:, LANES:]),
        (inner_hbm, inner), (outer_hbm.at[kv], outer), (wq_hbm, wq),
        (wo_hbm.at[pl.ds(tp * mine, mine)], wo.at[0]), (wo_hbm.at[pl.ds((1 - tp) * mine, mine)], wo.at[1]),
    ]
    loads = [pltpu.make_async_copy(a, b, load_sem.at[i]) for i, (a, b) in enumerate(pairs)]
    for load in loads:
        load.start()
    l_pick, l_doc, l_tok, l_wk, l_wv, l_in, l_out, l_wq, l_wo0, l_wo1 = loads

    l_pick.wait()
    slots = jnp.concatenate([pick[b] for b in range(blocks)], axis=0)
    block_ids = iota((blocks, wide), 1)
    hit = slots[:, 0:1] == block_ids
    for s in range(1, slots.shape[1]):
        hit = hit | (slots[:, s:s + 1] == block_ids)
    named_any = jnp.max(jnp.where(hit, 1.0, 0.0), axis=0, keepdims=True)
    names[...] = jnp.broadcast_to(named_any, names.shape)

    pl.semaphore_wait(barrier, before + after + 1)

    def name_copy(i):
        return pltpu.make_async_remote_copy(
            src_ref=names, dst_ref=names_in.at[i], send_sem=name_s.at[i], recv_sem=name_r.at[i],
            device_id={"kv": kv - 1 - i}, device_id_type=MESH)

    def name_send(i, _):
        name_copy(i).start()
        return 0

    lax.fori_loop(0, before, name_send, 0)

    def clear(i, _):
        hot_in[i] = jnp.zeros(hot_in.shape[1:], BF16)
        ids_in[i] = jnp.zeros(ids_in.shape[1:], F32)
        return 0

    lax.fori_loop(before, reach, clear, 0)

    l_in.wait()
    l_out.wait()
    cos_o, sin_o = outer[0:1, :], outer[1:2, :]
    cos_i, sin_i = inner[0], inner[1]
    cosine = cos_o * cos_i - sin_o * sin_i
    sine = sin_o * cos_i + cos_o * sin_i
    lane = iota((rows, LANES), 1)
    low = lane < HEAD_DIM
    first = lane % HEAD_DIM < HEAD_DIM // 2
    quarter = HEAD_DIM // 2

    def rotate(x):
        other = jnp.where(first, pltpu.roll(x, LANES - quarter, 1), pltpu.roll(x, quarter, 1))
        return x * cosine + other * sine

    def swap(x):
        return pltpu.roll(x, HEAD_DIM, 1)

    l_tok.wait()
    l_wk.wait()
    l_wv.wait()
    both = dot(tok[...], wkv[...])
    keys = rotate(both[:, 0:LANES])
    values = both[:, LANES:]
    is_first = tp == 0
    keys = jnp.where(is_first, keys, swap(keys))
    values = jnp.where(is_first, swap(values), values)
    packed = jnp.where(low, keys, values).astype(BF16)
    kv_own[...] = packed

    l_wq.wait()
    queries = dot(tok[...], wq[...])
    for p in range(heads // 2):
        turned = rotate(queries[:, p * LANES:(p + 1) * LANES])
        q_all[2 * p * rows:(2 * p + 1) * rows, :] = jnp.where(low, turned, 0.0).astype(BF16)
        q_all[(2 * p + 1) * rows:(2 * p + 2) * rows, :] = jnp.where(low, swap(turned), 0.0).astype(BF16)

    def name_take(i, total):
        name_copy(i).wait_recv()
        return total + names_in[i]

    total = lax.fori_loop(0, after, name_take, jnp.zeros(names.shape, F32))
    flags = jnp.broadcast_to(jnp.where(total > 0.0, 1.0, 0.0), (8, wide)).astype(BF16)
    j = iota((wide, rows), 0) - kv * blocks
    col = iota((wide, rows), 1) // BLOCK
    here = dot(flags, jnp.where(j == col, 1.0, 0.0).astype(BF16))[0:1, :]
    rank = dot(flags, jnp.where((j >= 0) & (j < col), 1.0, 0.0).astype(BF16))[0:1, :]
    kept = HOT * BLOCK
    slot = iota((2 * kept, rows), 0) % kept
    own = iota((2 * kept, rows), 1)
    choose = (here > 0.5) & (rank == (slot // BLOCK).astype(F32)) & (own % BLOCK == slot % BLOCK)
    choose = jnp.where(choose, 1.0, 0.0).astype(BF16)
    label = (iota((16, rows), 1) // BLOCK + 1).astype(F32).astype(BF16)
    pack[...] = dot(choose[0:kept], packed).astype(BF16)
    ids[...] = dot_t(label, choose)[0:1, :]

    def hot_copy(i):
        return pltpu.make_async_remote_copy(
            src_ref=pack, dst_ref=hot_in.at[i], send_sem=hot_s.at[i], recv_sem=hot_r.at[i],
            device_id={"kv": kv + 1 + i}, device_id_type=MESH)

    def ids_copy(i):
        return pltpu.make_async_remote_copy(
            src_ref=ids, dst_ref=ids_in.at[i], send_sem=ids_s.at[i], recv_sem=ids_r.at[i],
            device_id={"kv": kv + 1 + i}, device_id_type=MESH)

    def hot_send(i, _):
        ids_copy(i).start()
        hot_copy(i).start()
        return 0

    lax.fori_loop(0, after, hot_send, 0)

    l_doc.wait()
    q_pos = kv * rows + iota((rows, 1), 0)
    q_start = jnp.zeros((rows, 1), jnp.int32)
    end = jnp.int32(0)
    for i in range(doc.shape[1]):
        end = end + doc[0, i]
        q_start = jnp.where(q_pos >= end, end, q_start)

    def bias_of(key_block, key_pos):
        hits = slots[:, 0:1] == key_block
        for s in range(1, slots.shape[1]):
            hits = hits | (slots[:, s:s + 1] == key_block)
        allowed = jnp.where(hits, 0.0, -jnp.inf)
        parts = []
        for b in range(blocks):
            span = slice(b * BLOCK, (b + 1) * BLOCK)
            seen = (key_pos <= q_pos[span]) & (key_pos >= q_start[span])
            parts.append(jnp.where(seen, allowed[b:b + 1, :], -jnp.inf))
        return jnp.concatenate(parts, axis=0)

    def with_ones(block):
        return jnp.where(iota(block.shape, 1) < HEAD_DIM, jnp.ones((), BF16), block)

    local_col = iota((1, rows), 1)
    bias = bias_of(kv * blocks + local_col // BLOCK, kv * rows + local_col)
    both = jnp.concatenate([bias, bias], axis=0)
    ones_values = with_ones(packed)
    for p in range(heads // 2):
        span = slice(2 * p * rows, (2 * p + 2) * rows)
        scores = dot_t(q_all[span, :], packed) * SCALE + both
        highest = jnp.max(scores, axis=-1, keepdims=True)
        weights = jnp.exp2(scores - highest).astype(BF16)
        acc[span, :] = dot(weights, ones_values)
        top[span, :] = jnp.broadcast_to(highest, (2 * rows, LANES))

    def att_copy(h):
        return pltpu.make_async_remote_copy(
            src_ref=att.at[h], dst_ref=att_in.at[h], send_sem=att_s.at[h], recv_sem=att_r.at[h],
            device_id={"tp": 1 - tp}, device_id_type=MESH)

    def hot_wait(i, _):
        ids_copy(i).wait_recv()
        hot_copy(i).wait_recv()
        return 0

    lax.fori_loop(0, before, hot_wait, 0)
    near = math.gcd(reach, 8)
    width = att.shape[2]

    def group(g, last):
        start = g * near
        block = hot_in[pl.ds(start, near)].reshape(near * kept, LANES)
        upper = iota((1, LANES), 1) < kept
        found = []
        for i in range(0, near, 2):
            base = (kv - 1 - start - i) * blocks - 1
            even = ids_in[start + i].astype(jnp.int32)
            odd = ids_in[start + i + 1].astype(jnp.int32)
            even = jnp.where(even > 0, base + even, -2)
            odd = jnp.where(odd > 0, base - blocks + odd, -2)
            found.append(jnp.where(upper, even, odd))
        key_block = jnp.concatenate(found, axis=1)
        key_pos = key_block * BLOCK + iota((1, near * kept), 1) % BLOCK
        bias = bias_of(key_block, key_pos)
        both = jnp.concatenate([bias, bias], axis=0)
        ones_values = with_ones(block)
        for p in range(heads // 2):
            span = slice(2 * p * rows, (2 * p + 2) * rows)
            scores = dot_t(q_all[span, :], block) * SCALE + both
            before = top[span, :]
            highest = jnp.maximum(before, jnp.max(scores, axis=-1, keepdims=True))
            weights = jnp.exp2(scores - highest[:, 0:1]).astype(BF16)
            summed = acc[span, :] * jnp.exp2(before - highest) + dot(weights, ones_values)
            if not last:
                acc[span, :] = summed
                top[span, :] = highest
                continue
            even, odd = summed[0:rows], summed[rows:]
            above = jnp.where(low, swap(even), odd)
            below = jnp.where(low, even, swap(odd))
            half, place = divmod(p * LANES, width)
            att[half, :, place:place + LANES] = (above / below).astype(BF16)
            if place + LANES == width:
                att_copy(half).start()

    if reach > near:
        def step(g, _):
            group(g, False)
            return 0

        lax.fori_loop(0, reach // near - 1, step, 0)
    group(reach // near - 1, True)

    l_wo0.wait()
    halves = att.shape[0]
    columns = wo.shape[2]
    piece = columns // 4
    for c in range(4):
        cut = slice(c * piece, (c + 1) * piece)
        value = dot(att[0], wo[0, 0:width, cut])
        for h in range(1, halves):
            value += dot(att[h], wo[0, h * width:(h + 1) * width, cut])
        partial[:, cut] = value
    l_wo1.wait()
    for h in range(halves):
        att_copy(h).wait_recv()
    for c in range(4):
        cut = slice(c * piece, (c + 1) * piece)
        value = partial[:, cut]
        for h in range(halves):
            value += dot(att_in[h], wo[1, h * width:(h + 1) * width, cut])
        out[0, :, cut] = value.astype(BF16)

    def name_done(i, _):
        name_copy(i).wait_send()
        return 0

    def hot_done(i, _):
        ids_copy(i).wait_send()
        hot_copy(i).wait_send()
        return 0

    lax.fori_loop(0, before, name_done, 0)
    lax.fori_loop(0, after, hot_done, 0)
    for h in range(halves):
        att_copy(h).wait_send()


def solution(mesh):
    n = mesh.shape["kv"]

    def shards(tokens, doc_lengths, picked, w_query, w_key, w_value, w_out):
        _, rows, d = tokens.shape
        blocks = rows // BLOCK
        wide = -(-n * blocks // LANES) * LANES
        q_cols = w_query.shape[1]
        heads = q_cols // HEAD_DIM
        columns = w_out.shape[1]
        inner, outer = tables(rows, n)
        width = q_cols // 2
        dma = pltpu.SemaphoreType.DMA
        payload = HOT * BLOCK
        reach = min(n, (n * rows // 2 + rows - 2) // rows)
        reach += reach % 2
        operands = (tokens, doc_lengths, jnp.transpose(picked, (1, 0, 2)), w_query, w_key, w_value, w_out, inner, outer)
        operands = [pltpu.with_memory_space_constraint(jnp.asarray(x), pltpu.HBM) for x in operands]
        return pl.pallas_call(
            functools.partial(kernel, n, reach),
            out_shape=jax.ShapeDtypeStruct((1, rows, columns), BF16),
            in_specs=[pl.BlockSpec(memory_space=pltpu.HBM)] * 9,
            out_specs=pl.BlockSpec(memory_space=pltpu.VMEM),
            scratch_shapes=[
                pltpu.VMEM((rows, d), BF16),
                pltpu.SMEM(doc_lengths.shape, jnp.int32),
                pltpu.VMEM((blocks, 1, picked.shape[2]), jnp.int32),
                pltpu.VMEM(w_query.shape, BF16),
                pltpu.VMEM((d, 2 * LANES), BF16),
                pltpu.VMEM((2, w_out.shape[0] // 2, columns), BF16),
                pltpu.VMEM(inner.shape, F32),
                pltpu.VMEM(outer.shape[1:], F32),
                pltpu.VMEM((1, wide), F32),
                pltpu.VMEM((reach, 1, wide), F32),
                pltpu.VMEM((rows, LANES), BF16),
                pltpu.VMEM((payload, LANES), BF16),
                pltpu.VMEM((reach, payload, LANES), BF16),
                pltpu.VMEM((1, LANES), F32),
                pltpu.VMEM((reach, 1, LANES), F32),
                pltpu.VMEM((heads * rows, LANES), BF16),
                pltpu.VMEM((heads * rows, LANES), F32),
                pltpu.VMEM((heads * rows, LANES), F32),
                pltpu.VMEM((2, rows, width), BF16),
                pltpu.VMEM((2, rows, width), BF16),
                pltpu.VMEM((rows, columns), F32),
                dma((10,)), *[dma((reach,))] * 6, dma((2,)), dma((2,)),
            ],
            compiler_params=pltpu.CompilerParams(
                collective_id=0, has_side_effects=True, vmem_limit_bytes=24 * 1024 * 1024
            ),
        )(*operands)

    placed = (P("dp", "kv", None), P("dp", None), P("dp", "kv", None), P(None, "tp"), P(), P(), P())
    return jax.shard_map(
        shards, mesh=mesh, in_specs=placed, out_specs=P("dp", "kv", None), check_vma=False
    )
```

profile of v0, /device:TPU:17, one launch (start us, length us, event | category | flops | bytes accessed | tf_op | source)
XLA Modules:
  0.0 15.5 jit_solution(6945570612197262478)
XLA Ops:
  0.0 14.6 %shard_map.91 = bf16[1,192,2048]{2,1,0:T(8,128)(2,1)S(1)} custom-call(bf16[1,192,2048]{2,1,0:T(8,128)(2,1)} %tok_hbm.1, s32[1,8]{1,0:T(1,128)} %doc_hbm.1, s32[6,1,32]{2,1,0:T(1,128)} %bitcast.1, bf16[2048,512]{1,0:T(8,128)(2,1)} %wq_hbm.1, bf16[2048,128]{1,0:T(8,128)(2,1)} %wk_hbm.1, bf16[2048,128]{1,0:T(8,128)(2,1)} %wv_hbm.1, bf16[1024,2048]{1,0:T(8,128)(2,1)} %wo_hbm.1, ...), custom_call_target="tpu_custom_call" | custom-call | tf_op jit(solution)/shard_map/pallas_call | solution.py:333
  14.6 0.9 %copy.11 = bf16[1,192,2048]{2,1,0:T(8,128)(2,1)} copy(bf16[1,192,2048]{2,1,0:T(8,128)(2,1)S(1)} %shard_map.91) | data formatting | bytes 1572864
where the time goes:
time: 15.7 us; the launch traced here: 15.5 us
  Pallas kernels  14.6 us (93%)
  local copies, waits for them, and re-layouts  0.88 us (6%)
    pallas_call x1, Pallas kernels, shards(): pl.pallas_call(functools.partial(kernel, n, reach), out_shape=jax.ShapeDt...  14.6 us
    unnamed x1, local copies, waits for them, and re-layouts  0.88 us

commit v1 on v0

v1 whole, which is shorter than its diff:
```python
import functools
import math

import jax
import jax.numpy as jnp
import numpy as np
from jax import lax
from jax.experimental import pallas as pl
from jax.experimental.pallas import tpu as pltpu
from jax.sharding import PartitionSpec as P

HEAD_DIM = 64
BLOCK = 32
LANES = 128
SPAN = 64
HOT = 2
NEAR = 2
STEP = 2
CHUNK = 256
MESH = pl.DeviceIdType.MESH
SCALE = float(HEAD_DIM ** -0.5 * np.log2(np.e))
FAR_OFF = 1 << 30
F32 = jnp.float32
BF16 = jnp.bfloat16


def tables(rows, count):
    lane = np.arange(LANES)
    half = HEAD_DIM // 2
    inverse = (10000.0 ** (-(lane % half) / half)).astype(np.float32).astype(np.float64)
    sign = np.where(lane % HEAD_DIM < half, -1.0, 1.0)
    row = np.arange(rows)[:, None] * inverse
    start = (np.arange(count) * rows)[:, None] * inverse
    inner = np.stack([np.cos(row), np.sin(row) * sign]).astype(np.float32)
    outer = np.zeros((count, 8, LANES), np.float32)
    outer[:, 0] = np.cos(start)
    outer[:, 1] = np.sin(start) * sign
    return inner, outer


def iota(shape, axis):
    return lax.broadcasted_iota(jnp.int32, shape, axis)


def dot_t(a, b):
    return lax.dot_general(a, b, (((1,), (1,)), ((), ())), preferred_element_type=F32)


def dot(a, b):
    return jnp.dot(a, b, preferred_element_type=F32)


def swap(x):
    return pltpu.roll(x, HEAD_DIM, 1)


def kernel(
    n, near, far, tok_hbm, doc_hbm, pick_hbm, wq_hbm, wk_hbm, wv_hbm, wo_hbm, inner_hbm, outer_hbm, out,
    tok, doc, pick, wq, wkv, wo, inner, outer, names, names_in, kv_all, kv_own, near_in, near_keys, pack, hot_in,
    ids, ids_in, bias, vt, q_all, acc, top, att, att_in, partial,
    load_sem, name_s, name_r, near_s, near_r, hot_s, hot_r, ids_s, ids_r, att_s, att_r,
):
    kv = lax.axis_index("kv")
    tp = lax.axis_index("tp")
    rows = tok.shape[0]
    blocks = rows // BLOCK
    heads = wq.shape[1] // HEAD_DIM
    mine = wo.shape[1]
    pad = names.shape[1]
    kept = HOT * BLOCK
    lead = tp == 1

    before_near = jnp.minimum(kv, near)
    before_far = jnp.clip(kv - near, 0, far)
    after_near = jnp.minimum(n - 1 - kv, near)
    after_far = jnp.clip(n - 1 - kv - near, 0, far)
    names_out = jnp.where(lead, before_far, 0)
    hots_out = jnp.where(lead, after_far, 0)

    barrier = pltpu.get_barrier_semaphore()

    def greet_near(i, _):
        pl.semaphore_signal(barrier, inc=1, device_id={"kv": kv - 1 - i}, device_id_type=MESH)
        return 0

    def greet_far(i, _):
        pl.semaphore_signal(barrier, inc=1, device_id={"kv": kv + 1 + near + i}, device_id_type=MESH)
        return 0

    lax.fori_loop(0, before_near, greet_near, 0)
    lax.fori_loop(0, hots_out, greet_far, 0)
    pl.semaphore_signal(barrier, inc=1, device_id={"tp": 1 - tp}, device_id_type=MESH)

    pairs = [
        (pick_hbm, pick), (tok_hbm.at[0], tok), (wk_hbm, wkv.at[:, 0:LANES]), (wv_hbm, wkv.at[:, LANES:]),
        (inner_hbm, inner), (outer_hbm.at[kv], outer), (doc_hbm, doc), (wq_hbm, wq),
        (wo_hbm.at[pl.ds(tp * mine, mine)], wo.at[0]), (wo_hbm.at[pl.ds((1 - tp) * mine, mine)], wo.at[1]),
    ]
    loads = [pltpu.make_async_copy(a, b, load_sem.at[i]) for i, (a, b) in enumerate(pairs)]
    for load in loads:
        load.start()
    l_pick, l_tok, l_wk, l_wv, l_in, l_out, l_doc, l_wq, l_wo0, l_wo1 = loads

    def clear_near(i, _):
        near_in[i] = jnp.zeros(near_in.shape[1:], BF16)
        return 0

    def clear_far(i, _):
        hot_in[i] = jnp.zeros(hot_in.shape[1:], BF16)
        ids_in[i] = jnp.zeros(ids_in.shape[1:], F32)
        return 0

    lax.fori_loop(before_near, near, clear_near, 0)
    lax.fori_loop(before_far, far, clear_far, 0)

    l_pick.wait()
    reach = near + far
    slot_rows = [pick[b] for b in range(blocks)]
    index = iota((reach * pad, slot_rows[0].shape[1]), 0)
    owner = kv - 1 - index // pad
    wanted = jnp.where((owner >= 0) & (index % pad < blocks), owner * blocks + index % pad, -9)
    hit = slot_rows[0] == wanted
    for b in range(1, blocks):
        hit = hit | (slot_rows[b] == wanted)
    flags = jnp.max(jnp.where(hit, 1.0, 0.0), axis=1, keepdims=True)
    names[...] = jnp.broadcast_to(flags, (reach * pad, LANES)).reshape(names.shape)

    l_in.wait()
    l_out.wait()
    cos_o, sin_o = outer[0:1, :], outer[1:2, :]
    cos_i, sin_i = inner[0], inner[1]
    cosine = cos_o * cos_i - sin_o * sin_i
    sine = sin_o * cos_i + cos_o * sin_i
    lane = iota((rows, LANES), 1)
    low = lane < HEAD_DIM
    first = lane % HEAD_DIM < HEAD_DIM // 2
    quarter = HEAD_DIM // 2

    def rotate(x):
        other = jnp.where(first, pltpu.roll(x, LANES - quarter, 1), pltpu.roll(x, quarter, 1))
        return x * cosine + other * sine

    l_tok.wait()
    l_wk.wait()
    l_wv.wait()
    both = dot(tok[...], wkv[...])
    keys = rotate(both[:, 0:LANES])
    values = both[:, LANES:]
    kv_all[0] = jnp.where(low, keys, swap(values))
    kv_all[1] = jnp.where(low, swap(keys), values)
    kv_own[...] = kv_all[tp].astype(BF16)

    pl.semaphore_wait(barrier, after_near + names_out + 1)

    def name_copy(i):
        return pltpu.make_async_remote_copy(
            src_ref=names.at[near + i], dst_ref=names_in.at[i], send_sem=name_s.at[i], recv_sem=name_r.at[i],
            device_id={"kv": kv - 1 - near - i}, device_id_type=MESH)

    def near_copy(i):
        return pltpu.make_async_remote_copy(
            src_ref=kv_own, dst_ref=near_in.at[i], send_sem=near_s.at[i], recv_sem=near_r.at[i],
            device_id={"kv": kv + 1 + i}, device_id_type=MESH)

    def hot_copy(i, t):
        return pltpu.make_async_remote_copy(
            src_ref=pack.at[t], dst_ref=hot_in.at[i], send_sem=hot_s.at[i, t], recv_sem=hot_r.at[i],
            device_id={"kv": kv + 1 + near + i, "tp": t}, device_id_type=MESH)

    def ids_copy(i, t):
        return pltpu.make_async_remote_copy(
            src_ref=ids, dst_ref=ids_in.at[i], send_sem=ids_s.at[i, t], recv_sem=ids_r.at[i],
            device_id={"kv": kv + 1 + near + i, "tp": t}, device_id_type=MESH)

    def name_send(i, _):
        name_copy(i).start()
        return 0

    def near_send(i, _):
        near_copy(i).start()
        return 0

    lax.fori_loop(0, names_out, name_send, 0)
    lax.fori_loop(0, after_near, near_send, 0)

    l_wq.wait()
    queries = dot(tok[...], wq[...])
    spans = rows // SPAN
    for p in range(heads // 2):
        turned = rotate(queries[:, p * LANES:(p + 1) * LANES])
        even = jnp.where(low, turned, 0.0).astype(BF16)
        odd = jnp.where(low, swap(turned), 0.0).astype(BF16)
        for r in range(spans):
            base = (p * spans + r) * LANES
            q_all[base:base + SPAN, :] = even[r * SPAN:(r + 1) * SPAN]
            q_all[base + SPAN:base + LANES, :] = odd[r * SPAN:(r + 1) * SPAN]

    l_doc.wait()
    tile_lane = iota((1, LANES), 1) % SPAN
    upper = iota((8, LANES), 1) % SPAN >= BLOCK
    q_pos = [kv * rows + r * SPAN + tile_lane for r in range(spans)]
    q_start = [jnp.zeros((1, LANES), jnp.int32) for _ in range(spans)]
    end = jnp.int32(0)
    for i in range(doc.shape[1]):
        end = end + doc[0, i]
        q_start = [jnp.where(pos >= end, end, s) for pos, s in zip(q_pos, q_start)]
    place = iota((BLOCK, LANES), 0)

    def set_bias(key_block, count, causal):
        found = []
        for b in range(blocks):
            same = slot_rows[b] == key_block[:, 0:slot_rows[b].shape[1]]
            found.append(jnp.max(jnp.where(same, 1.0, 0.0), axis=1, keepdims=True))
        for r in range(spans):
            named = jnp.where(upper, found[2 * r + 1], found[2 * r])
            floor = jnp.where(named > 0.5, q_start[r] - key_block * BLOCK, FAR_OFF)
            for k in range(count):
                live = place >= floor[k:k + 1, :]
                if causal:
                    live = live & (place <= q_pos[r] - (kv * rows + k * BLOCK))
                bias[k * BLOCK:(k + 1) * BLOCK, r * LANES:(r + 1) * LANES] = jnp.where(live, 0.0, -jnp.inf)

    def set_values(block):
        count = block.shape[0]
        vt[0:HEAD_DIM, 0:count] = jnp.transpose(block.astype(F32))[HEAD_DIM:, :].astype(BF16)

    def score(c, block):
        return dot_t(block, q_all[c * CHUNK:(c + 1) * CHUNK, :])

    def absorb(c, scores, fresh):
        count = scores.shape[0]
        cut = slice(c * CHUNK, (c + 1) * CHUNK)
        tiles = []
        for t in range(CHUNK // LANES):
            r = (c * (CHUNK // LANES) + t) % spans
            tiles.append(scores[:, t * LANES:(t + 1) * LANES] + bias[0:count, r * LANES:(r + 1) * LANES])
        scores = jnp.concatenate(tiles, axis=1)
        highest = jnp.max(scores, axis=0, keepdims=True)
        if not fresh:
            old = top[:, cut]
            highest = jnp.maximum(highest, old)
        weights = jnp.exp2((scores - highest) * SCALE).astype(BF16)
        summed = dot(vt[:, 0:count], weights)
        if not fresh:
            summed = summed + acc[:, cut] * jnp.exp2((old - highest) * SCALE)
        acc[:, cut] = summed
        top[:, cut] = highest

    def attend(begin, stop, block, fresh, after=None):
        ready = score(begin, block)
        for c in range(begin, stop):
            now = ready
            if c + 1 < stop:
                ready = score(c + 1, block)
            absorb(c, now, fresh)
            if after is not None:
                after(c)

    chunks = heads * rows // CHUNK
    vt[HEAD_DIM:, :] = jnp.ones((vt.shape[0] - HEAD_DIM, vt.shape[1]), BF16)
    local_block = iota((8, LANES), 0)
    set_bias(jnp.where(local_block < blocks, kv * blocks + local_block, -2), blocks, True)
    set_values(kv_all[tp])
    own = kv_own[...]
    attend(0, chunks, own, True)

    def choose(flag, base):
        rank = jnp.zeros((1, LANES), F32)
        weight = [[], []]
        label = [jnp.zeros((1, LANES), F32) for _ in range(HOT)]
        for b in range(blocks):
            for s in range(HOT):
                one = jnp.where((flag[b] > 0.5) & (rank == s), 1.0, 0.0)
                weight[s].append(one)
                label[s] = label[s] + one * (b + 1)
            rank = rank + flag[b]
        return weight, label

    def gather(weight, block):
        total = block(0) * weight[0]
        for b in range(1, blocks):
            total = total + block(b) * weight[b]
        return total

    @pl.when(lead)
    def _():
        def name_take(i, total):
            name_copy(i).wait_recv()
            return total + names_in[i]

        total = lax.fori_loop(0, after_far, name_take, jnp.zeros(names.shape[1:], F32))
        total = jnp.where(total > 0.5, 1.0, 0.0)
        weight, label = choose([total[b:b + 1, :] for b in range(blocks)], 0)
        for s in range(HOT):
            ids[s:s + 1, :] = label[s]
            for t in range(2):
                part = gather(weight[s], lambda b: kv_all[t, b * BLOCK:(b + 1) * BLOCK, :])
                pack[t, s * BLOCK:(s + 1) * BLOCK, :] = part.astype(BF16)

        def hot_send(i, _):
            for t in range(2):
                ids_copy(i, t).start()
            for t in range(2):
                hot_copy(i, t).start()
            return 0

        lax.fori_loop(0, after_far, hot_send, 0)

    def near_wait(i, _):
        near_copy(i).wait_recv()
        return 0

    def key_blocks(labels):
        found = [jnp.where(v > 0.5, base + v.astype(jnp.int32) - 1, -2) for base, v in labels]
        found += [jnp.full((1, LANES), -2, jnp.int32)] * (8 - len(found))
        return jnp.concatenate(found, axis=0)

    chosen = [choose([names[i, b:b + 1, :] for b in range(blocks)], 0) for i in range(near)]
    set_bias(key_blocks([((kv - 1 - i) * blocks, v) for i in range(near) for v in chosen[i][1]]), near * HOT, False)
    lax.fori_loop(0, before_near, near_wait, 0)
    for i in range(near):
        for s in range(HOT):
            part = gather(chosen[i][0][s], lambda b: near_in[i, b * BLOCK:(b + 1) * BLOCK, :].astype(F32))
            at = (i * HOT + s) * BLOCK
            near_keys[at:at + BLOCK, :] = part.astype(BF16)
    block = near_keys[...]
    set_values(block)
    attend(0, chunks, block, False)

    def att_copy(h):
        return pltpu.make_async_remote_copy(
            src_ref=att.at[h], dst_ref=att_in.at[h], send_sem=att_s.at[h], recv_sem=att_r.at[h],
            device_id={"tp": 1 - tp}, device_id_type=MESH)

    def ids_wait(i, _):
        ids_copy(i, tp).wait_recv()
        return 0

    def hot_wait(i, _):
        hot_copy(i, tp).wait_recv()
        return 0

    lax.fori_loop(0, before_far, ids_wait, 0)
    width = att.shape[2]
    halves = att.shape[0]

    def far_bias(start):
        labels = [((kv - 1 - near - start - i) * blocks, ids_in[start + i, s:s + 1, :]) for i in range(STEP) for s in range(HOT)]
        set_bias(key_blocks(labels), STEP * HOT, False)

    def far_block(start):
        block = hot_in[pl.ds(start, STEP)].reshape(STEP * kept, LANES)
        set_values(block)
        return block

    steps = far // STEP
    if steps > 1:
        lax.fori_loop(0, before_far, hot_wait, 0)

        def far_step(g, _):
            far_bias(g * STEP)
            block = far_block(g * STEP)
            attend(0, chunks, block, False)
            return 0

        lax.fori_loop(0, steps - 1, far_step, 0)
    far_bias((steps - 1) * STEP)
    if steps == 1:
        lax.fori_loop(0, before_far, hot_wait, 0)
    block = far_block((steps - 1) * STEP)
    low_tile = iota((SPAN, LANES), 1) < HEAD_DIM

    def finish(c):
        if (c + 1) * halves % chunks:
            return
        h = (c + 1) * halves // chunks - 1
        for p in range(h * heads // 2 // halves, (h + 1) * heads // 2 // halves):
            for r in range(spans):
                t = p * spans + r
                cut = slice(t * LANES, (t + 1) * LANES)
                part = acc[0:HEAD_DIM, cut] * (1.0 / acc[HEAD_DIM:HEAD_DIM + 1, cut])
                turned = jnp.transpose(jnp.concatenate([part, part], axis=0))
                part = jnp.where(low_tile, turned[0:SPAN], turned[SPAN:])
                at = p * LANES - h * width
                att[h, r * SPAN:(r + 1) * SPAN, at:at + LANES] = part.astype(BF16)
        att_copy(h).start()

    attend(0, chunks, block, False, finish)

    l_wo0.wait()
    columns = wo.shape[2]
    piece = columns // 4
    for c in range(4):
        cut = slice(c * piece, (c + 1) * piece)
        value = dot(att[0], wo[0, 0:width, cut])
        for h in range(1, halves):
            value += dot(att[h], wo[0, h * width:(h + 1) * width, cut])
        partial[:, cut] = value
    l_wo1.wait()
    for h in range(halves):
        att_copy(h).wait_recv()
    for c in range(4):
        cut = slice(c * piece, (c + 1) * piece)
        value = partial[:, cut]
        for h in range(halves):
            value += dot(att_in[h], wo[1, h * width:(h + 1) * width, cut])
        out[0, :, cut] = value.astype(BF16)

    def name_done(i, _):
        name_copy(i).wait_send()
        return 0

    def near_done(i, _):
        near_copy(i).wait_send()
        return 0

    def hot_done(i, _):
        for t in range(2):
            ids_copy(i, t).wait_send()
            hot_copy(i, t).wait_send()
        return 0

    lax.fori_loop(0, names_out, name_done, 0)
    lax.fori_loop(0, after_near, near_done, 0)
    lax.fori_loop(0, hots_out, hot_done, 0)
    for h in range(halves):
        att_copy(h).wait_send()


def solution(mesh):
    n = mesh.shape["kv"]

    def shards(tokens, doc_lengths, picked, w_query, w_key, w_value, w_out):
        _, rows, d = tokens.shape
        blocks = rows // BLOCK
        pad = -(-blocks // 8) * 8
        q_cols = w_query.shape[1]
        heads = q_cols // HEAD_DIM
        columns = w_out.shape[1]
        inner, outer = tables(rows, n)
        width = q_cols // 2
        dma = pltpu.SemaphoreType.DMA
        payload = HOT * BLOCK
        reach = min(n, (n * rows // 2 + rows - 2) // rows)
        near = NEAR
        far = -(-max(reach - near, 1) // STEP) * STEP
        most = max(rows, near * payload, STEP * payload)
        operands = (tokens, doc_lengths, jnp.transpose(picked, (1, 0, 2)), w_query, w_key, w_value, w_out, inner, outer)
        operands = [pltpu.with_memory_space_constraint(jnp.asarray(x), pltpu.HBM) for x in operands]
        return pl.pallas_call(
            functools.partial(kernel, n, near, far),
            out_shape=jax.ShapeDtypeStruct((1, rows, columns), BF16),
            in_specs=[pl.BlockSpec(memory_space=pltpu.HBM)] * 9,
            out_specs=pl.BlockSpec(memory_space=pltpu.VMEM),
            scratch_shapes=[
                pltpu.VMEM((rows, d), BF16),
                pltpu.SMEM(doc_lengths.shape, jnp.int32),
                pltpu.VMEM((blocks, 1, picked.shape[2]), jnp.int32),
                pltpu.VMEM(w_query.shape, BF16),
                pltpu.VMEM((d, 2 * LANES), BF16),
                pltpu.VMEM((2, w_out.shape[0] // 2, columns), BF16),
                pltpu.VMEM(inner.shape, F32),
                pltpu.VMEM(outer.shape[1:], F32),
                pltpu.VMEM((near + far, pad, LANES), F32),
                pltpu.VMEM((far, pad, LANES), F32),
                pltpu.VMEM((2, rows, LANES), F32),
                pltpu.VMEM((rows, LANES), BF16),
                pltpu.VMEM((near, rows, LANES), BF16),
                pltpu.VMEM((near * payload, LANES), BF16),
                pltpu.VMEM((2, payload, LANES), BF16),
                pltpu.VMEM((far, payload, LANES), BF16),
                pltpu.VMEM((HOT, LANES), F32),
                pltpu.VMEM((far, HOT, LANES), F32),
                pltpu.VMEM((most, rows // SPAN * LANES), F32),
                pltpu.VMEM((HEAD_DIM + 16, most), BF16),
                pltpu.VMEM((heads * rows, LANES), BF16),
                pltpu.VMEM((HEAD_DIM + 16, heads * rows), F32),
                pltpu.VMEM((1, heads * rows), F32),
                pltpu.VMEM((2, rows, width), BF16),
                pltpu.VMEM((2, rows, width), BF16),
                pltpu.VMEM((rows, columns), F32),
                dma((10,)), dma((far,)), dma((far,)), dma((near,)), dma((near,)),
                dma((far, 2)), dma((far,)), dma((far, 2)), dma((far,)), dma((2,)), dma((2,)),
            ],
            compiler_params=pltpu.CompilerParams(
                collective_id=0, has_side_effects=True, vmem_limit_bytes=28 * 1024 * 1024
            ),
        )(*operands)

    placed = (P("dp", "kv", None), P("dp", None), P("dp", "kv", None), P(None, "tp"), P(), P(), P())
    return jax.shard_map(
        shards, mesh=mesh, in_specs=placed, out_specs=P("dp", "kv", None), check_vma=False
    )
```

time: 15.7 us -> 13 us (0.83)
  the two profiles are of different devices: /device:TPU:17 before, /device:TPU:25 now
where the time goes in v1:
time: 13 us; the launch traced here: 12.8 us
  Pallas kernels  11.9 us (92%)
  local copies, waits for them, and re-layouts  0.88 us (7%)
    pallas_call x1, Pallas kernels, shards(): pl.pallas_call(functools.partial(kernel, n, near, far), out_shape=jax.Sha...  11.9 us
    unnamed x1, local copies, waits for them, and re-layouts  0.88 us

profile of v1, /device:TPU:25, one launch (start us, length us, event | category | flops | bytes accessed | tf_op | source)
XLA Modules:
  0.0 12.8 jit_solution(16873821576055248837)
XLA Ops:
  0.0 11.9 %shard_map.91 = bf16[1,192,2048]{2,1,0:T(8,128)(2,1)S(1)} custom-call(bf16[1,192,2048]{2,1,0:T(8,128)(2,1)} %tok_hbm.1, s32[1,8]{1,0:T(1,128)} %doc_hbm.1, s32[6,1,32]{2,1,0:T(1,128)} %bitcast.1, bf16[2048,512]{1,0:T(8,128)(2,1)} %wq_hbm.1, bf16[2048,128]{1,0:T(8,128)(2,1)} %wk_hbm.1, bf16[2048,128]{1,0:T(8,128)(2,1)} %wv_hbm.1, bf16[1024,2048]{1,0:T(8,128)(2,1)} %wo_hbm.1, ...), custom_call_target="tpu_custom_call" | custom-call | tf_op jit(solution)/shard_map/pallas_call | solution.py:450
  11.9 0.9 %copy.11 = bf16[1,192,2048]{2,1,0:T(8,128)(2,1)} copy(bf16[1,192,2048]{2,1,0:T(8,128)(2,1)S(1)} %shard_map.91) | data formatting | bytes 1572864

commit v2 on v1

--- a/solution.py
+++ b/solution.py
@@ -125,6 +125,38 @@
     flags = jnp.max(jnp.where(hit, 1.0, 0.0), axis=1, keepdims=True)
     names[...] = jnp.broadcast_to(flags, (reach * pad, LANES)).reshape(names.shape)
 
+    pl.semaphore_wait(barrier, after_near + names_out + 1)
+
+    def name_copy(i):
+        return pltpu.make_async_remote_copy(
+            src_ref=names.at[near + i], dst_ref=names_in.at[i], send_sem=name_s.at[i], recv_sem=name_r.at[i],
+            device_id={"kv": kv - 1 - near - i}, device_id_type=MESH)
+
+    def near_copy(i):
+        return pltpu.make_async_remote_copy(
+            src_ref=kv_own, dst_ref=near_in.at[i], send_sem=near_s.at[i], recv_sem=near_r.at[i],
+            device_id={"kv": kv + 1 + i}, device_id_type=MESH)
+
+    def hot_copy(i, t):
+        return pltpu.make_async_remote_copy(
+            src_ref=pack.at[t], dst_ref=hot_in.at[i], send_sem=hot_s.at[i, t], recv_sem=hot_r.at[i],
+            device_id={"kv": kv + 1 + near + i, "tp": t}, device_id_type=MESH)
+
+    def ids_copy(i, t):
+        return pltpu.make_async_remote_copy(
+            src_ref=ids, dst_ref=ids_in.at[i], send_sem=ids_s.at[i, t], recv_sem=ids_r.at[i],
+            device_id={"kv": kv + 1 + near + i, "tp": t}, device_id_type=MESH)
+
+    def name_send(i, _):
+        name_copy(i).start()
+        return 0
+
+    def near_send(i, _):
+        near_copy(i).start()
+        return 0
+
+    lax.fori_loop(0, names_out, name_send, 0)
+
     l_in.wait()
     l_out.wait()
     cos_o, sin_o = outer[0:1, :], outer[1:2, :]
@@ -150,56 +182,34 @@
     kv_all[1] = jnp.where(low, swap(keys), values)
     kv_own[...] = kv_all[tp].astype(BF16)
 
-    pl.semaphore_wait(barrier, after_near + names_out + 1)
-
-    def name_copy(i):
-        return pltpu.make_async_remote_copy(
-            src_ref=names.at[near + i], dst_ref=names_in.at[i], send_sem=name_s.at[i], recv_sem=name_r.at[i],
-            device_id={"kv": kv - 1 - near - i}, device_id_type=MESH)
-
-    def near_copy(i):
-        return pltpu.make_async_remote_copy(
-            src_ref=kv_own, dst_ref=near_in.at[i], send_sem=near_s.at[i], recv_sem=near_r.at[i],
-            device_id={"kv": kv + 1 + i}, device_id_type=MESH)
-
-    def hot_copy(i, t):
-        return pltpu.make_async_remote_copy(
-            src_ref=pack.at[t], dst_ref=hot_in.at[i], send_sem=hot_s.at[i, t], recv_sem=hot_r.at[i],
-            device_id={"kv": kv + 1 + near + i, "tp": t}, device_id_type=MESH)
-
-    def ids_copy(i, t):
-        return pltpu.make_async_remote_copy(
-            src_ref=ids, dst_ref=ids_in.at[i], send_sem=ids_s.at[i, t], recv_sem=ids_r.at[i],
-            device_id={"kv": kv + 1 + near + i, "tp": t}, device_id_type=MESH)
-
-    def name_send(i, _):
-        name_copy(i).start()
-        return 0
-
-    def near_send(i, _):
-        near_copy(i).start()
-        return 0
-
-    lax.fori_loop(0, names_out, name_send, 0)
     lax.fori_loop(0, after_near, near_send, 0)
-
     l_wq.wait()
     queries = dot(tok[...], wq[...])
-    spans = rows // SPAN
+    main = rows // LANES
+    tail = rows % LANES
+    kinds = [m for m in range(main) for _ in range(2)] + [main] * (tail > 0)
+    per = len(kinds)
     for p in range(heads // 2):
         turned = rotate(queries[:, p * LANES:(p + 1) * LANES])
-        even = jnp.where(low, turned, 0.0).astype(BF16)
-        odd = jnp.where(low, swap(turned), 0.0).astype(BF16)
-        for r in range(spans):
-            base = (p * spans + r) * LANES
-            q_all[base:base + SPAN, :] = even[r * SPAN:(r + 1) * SPAN]
-            q_all[base + SPAN:base + LANES, :] = odd[r * SPAN:(r + 1) * SPAN]
+        flat = jnp.transpose(turned[0:main * LANES])
+        for m in range(main):
+            for e in range(2):
+                at = (p * per + 2 * m + e) * LANES
+                part = flat[e * HEAD_DIM:(e + 1) * HEAD_DIM, m * LANES:(m + 1) * LANES]
+                q_all[:, at:at + LANES] = part.astype(BF16)
+        if tail:
+            rest = turned[main * LANES:]
+            both = jnp.transpose(jnp.concatenate([rest, swap(rest)], axis=0))
+            at = (p * per + per - 1) * LANES
+            q_all[:, at:at + LANES] = both[0:HEAD_DIM].astype(BF16)
 
     l_doc.wait()
-    tile_lane = iota((1, LANES), 1) % SPAN
-    upper = iota((8, LANES), 1) % SPAN >= BLOCK
-    q_pos = [kv * rows + r * SPAN + tile_lane for r in range(spans)]
-    q_start = [jnp.zeros((1, LANES), jnp.int32) for _ in range(spans)]
+    lane_row = iota((1, LANES), 1)
+    wide_row = iota((8, LANES), 1)
+    q_row = [m * LANES + lane_row for m in range(main)] + [main * LANES + lane_row % SPAN] * (tail > 0)
+    wide_q = [m * LANES + wide_row for m in range(main)] + [main * LANES + wide_row % SPAN] * (tail > 0)
+    q_pos = [kv * rows + row for row in q_row]
+    q_start = [jnp.zeros((1, LANES), jnp.int32) for _ in q_row]
     end = jnp.int32(0)
     for i in range(doc.shape[1]):
         end = end + doc[0, i]
@@ -211,8 +221,12 @@
         for b in range(blocks):
             same = slot_rows[b] == key_block[:, 0:slot_rows[b].shape[1]]
             found.append(jnp.max(jnp.where(same, 1.0, 0.0), axis=1, keepdims=True))
-        for r in range(spans):
-            named = jnp.where(upper, found[2 * r + 1], found[2 * r])
+        for r in range(len(q_row)):
+            begin = r * LANES // BLOCK
+            stop = min(begin + LANES // BLOCK, blocks)
+            named = found[begin]
+            for b in range(begin + 1, stop):
+                named = jnp.where(wide_q[r] >= b * BLOCK, found[b], named)
             floor = jnp.where(named > 0.5, q_start[r] - key_block * BLOCK, FAR_OFF)
             for k in range(count):
                 live = place >= floor[k:k + 1, :]
@@ -225,14 +239,14 @@
         vt[0:HEAD_DIM, 0:count] = jnp.transpose(block.astype(F32))[HEAD_DIM:, :].astype(BF16)
 
     def score(c, block):
-        return dot_t(block, q_all[c * CHUNK:(c + 1) * CHUNK, :])
+        return dot(block[:, 0:HEAD_DIM], q_all[:, c * CHUNK:(c + 1) * CHUNK])
 
     def absorb(c, scores, fresh):
         count = scores.shape[0]
         cut = slice(c * CHUNK, (c + 1) * CHUNK)
         tiles = []
         for t in range(CHUNK // LANES):
-            r = (c * (CHUNK // LANES) + t) % spans
+            r = kinds[(c * (CHUNK // LANES) + t) % per]
             tiles.append(scores[:, t * LANES:(t + 1) * LANES] + bias[0:count, r * LANES:(r + 1) * LANES])
         scores = jnp.concatenate(tiles, axis=1)
         highest = jnp.max(scores, axis=0, keepdims=True)
@@ -375,14 +389,20 @@
             return
         h = (c + 1) * halves // chunks - 1
         for p in range(h * heads // 2 // halves, (h + 1) * heads // 2 // halves):
-            for r in range(spans):
-                t = p * spans + r
-                cut = slice(t * LANES, (t + 1) * LANES)
-                part = acc[0:HEAD_DIM, cut] * (1.0 / acc[HEAD_DIM:HEAD_DIM + 1, cut])
+            at = p * LANES - h * width
+
+            def scaled(t):
+                cut = slice((p * per + t) * LANES, (p * per + t + 1) * LANES)
+                return acc[0:HEAD_DIM, cut] * (1.0 / acc[HEAD_DIM:HEAD_DIM + 1, cut])
+
+            for m in range(main):
+                part = jnp.transpose(jnp.concatenate([scaled(2 * m), scaled(2 * m + 1)], axis=0))
+                att[h, m * LANES:(m + 1) * LANES, at:at + LANES] = part.astype(BF16)
+            if tail:
+                part = scaled(per - 1)
                 turned = jnp.transpose(jnp.concatenate([part, part], axis=0))
                 part = jnp.where(low_tile, turned[0:SPAN], turned[SPAN:])
-                at = p * LANES - h * width
-                att[h, r * SPAN:(r + 1) * SPAN, at:at + LANES] = part.astype(BF16)
+                att[h, main * LANES:, at:at + LANES] = part.astype(BF16)
         att_copy(h).start()
 
     attend(0, chunks, block, False, finish)
@@ -397,13 +417,17 @@
             value += dot(att[h], wo[0, h * width:(h + 1) * width, cut])
         partial[:, cut] = value
     l_wo1.wait()
-    for h in range(halves):
-        att_copy(h).wait_recv()
+    att_copy(0).wait_recv()
+    for h in range(halves - 1):
+        if h:
+            att_copy(h).wait_recv()
+        for c in range(4):
+            cut = slice(c * piece, (c + 1) * piece)
+            partial[:, cut] += dot(att_in[h], wo[1, h * width:(h + 1) * width, cut])
+    att_copy(halves - 1).wait_recv()
     for c in range(4):
         cut = slice(c * piece, (c + 1) * piece)
-        value = partial[:, cut]
-        for h in range(halves):
-            value += dot(att_in[h], wo[1, h * width:(h + 1) * width, cut])
+        value = partial[:, cut] + dot(att_in[halves - 1], wo[1, (halves - 1) * width:halves * width, cut])
         out[0, :, cut] = value.astype(BF16)
 
     def name_done(i, _):
@@ -471,9 +495,9 @@
                 pltpu.VMEM((far, payload, LANES), BF16),
                 pltpu.VMEM((HOT, LANES), F32),
                 pltpu.VMEM((far, HOT, LANES), F32),
-                pltpu.VMEM((most, rows // SPAN * LANES), F32),
+                pltpu.VMEM((most, -(-rows // LANES) * LANES), F32),
                 pltpu.VMEM((HEAD_DIM + 16, most), BF16),
-                pltpu.VMEM((heads * rows, LANES), BF16),
+                pltpu.VMEM((HEAD_DIM, heads * rows), BF16),
                 pltpu.VMEM((HEAD_DIM + 16, heads * rows), F32),
                 pltpu.VMEM((1, heads * rows), F32),
                 pltpu.VMEM((2, rows, width), BF16),

time: 13 us -> 11.8 us (0.908)
  Pallas kernels: 11.9 us -> 10.7 us
    pallas_call x1, Pallas kernels: 11.9 us -> 10.7 us  [shards(): pl.pallas_call(functools.partial(kernel, n, near, far), out_shape=jax.Sha...]
where the time goes in v2:
time: 11.8 us; the launch traced here: 11.6 us
  Pallas kernels  10.7 us (91%)
  local copies, waits for them, and re-layouts  0.88 us (7%)
    pallas_call x1, Pallas kernels, shards(): pl.pallas_call(functools.partial(kernel, n, near, far), out_shape=jax.Sha...  10.7 us
    unnamed x1, local copies, waits for them, and re-layouts  0.88 us

profile of v2, /device:TPU:25, one launch (start us, length us, event | category | flops | bytes accessed | tf_op | source)
XLA Modules:
  0.0 11.6 jit_solution(3882231531570808790)
XLA Ops:
  0.0 10.7 %shard_map.91 = bf16[1,192,2048]{2,1,0:T(8,128)(2,1)S(1)} custom-call(bf16[1,192,2048]{2,1,0:T(8,128)(2,1)} %tok_hbm.1, s32[1,8]{1,0:T(1,128)} %doc_hbm.1, s32[6,1,32]{2,1,0:T(1,128)} %bitcast.1, bf16[2048,512]{1,0:T(8,128)(2,1)} %wq_hbm.1, bf16[2048,128]{1,0:T(8,128)(2,1)} %wk_hbm.1, bf16[2048,128]{1,0:T(8,128)(2,1)} %wv_hbm.1, bf16[1024,2048]{1,0:T(8,128)(2,1)} %wo_hbm.1, ...), custom_call_target="tpu_custom_call" | custom-call | tf_op jit(solution)/shard_map/pallas_call | solution.py:474
  10.7 0.9 %copy.11 = bf16[1,192,2048]{2,1,0:T(8,128)(2,1)} copy(bf16[1,192,2048]{2,1,0:T(8,128)(2,1)S(1)} %shard_map.91) | data formatting | bytes 1572864

commit v3 on v2

--- a/solution.py
+++ b/solution.py
@@ -17,6 +17,7 @@
 NEAR = 2
 STEP = 2
 CHUNK = 256
+DEPTH = 6
 MESH = pl.DeviceIdType.MESH
 SCALE = float(HEAD_DIM ** -0.5 * np.log2(np.e))
 FAR_OFF = 1 << 30
@@ -57,8 +58,8 @@
 def kernel(
     n, near, far, tok_hbm, doc_hbm, pick_hbm, wq_hbm, wk_hbm, wv_hbm, wo_hbm, inner_hbm, outer_hbm, out,
     tok, doc, pick, wq, wkv, wo, inner, outer, names, names_in, kv_all, kv_own, near_in, near_keys, pack, hot_in,
-    ids, ids_in, bias, vt, q_all, acc, top, att, att_in, partial,
-    load_sem, name_s, name_r, near_s, near_r, hot_s, hot_r, ids_s, ids_r, att_s, att_r,
+    bias, vt, q_all, acc, top, att, att_in, partial,
+    load_sem, name_s, name_r, near_s, near_r, hot_s, hot_r, att_s, att_r,
 ):
     kv = lax.axis_index("kv")
     tp = lax.axis_index("tp")
@@ -107,7 +108,6 @@
 
     def clear_far(i, _):
         hot_in[i] = jnp.zeros(hot_in.shape[1:], BF16)
-        ids_in[i] = jnp.zeros(ids_in.shape[1:], F32)
         return 0
 
     lax.fori_loop(before_near, near, clear_near, 0)
@@ -139,12 +139,7 @@
 
     def hot_copy(i, t):
         return pltpu.make_async_remote_copy(
-            src_ref=pack.at[t], dst_ref=hot_in.at[i], send_sem=hot_s.at[i, t], recv_sem=hot_r.at[i],
-            device_id={"kv": kv + 1 + near + i, "tp": t}, device_id_type=MESH)
-
-    def ids_copy(i, t):
-        return pltpu.make_async_remote_copy(
-            src_ref=ids, dst_ref=ids_in.at[i], send_sem=ids_s.at[i, t], recv_sem=ids_r.at[i],
+            src_ref=pack.at[i, t], dst_ref=hot_in.at[i], send_sem=hot_s.at[i, t], recv_sem=hot_r.at[i],
             device_id={"kv": kv + 1 + near + i, "tp": t}, device_id_type=MESH)
 
     def name_send(i, _):
@@ -236,7 +231,7 @@
 
     def set_values(block):
         count = block.shape[0]
-        vt[0:HEAD_DIM, 0:count] = jnp.transpose(block.astype(F32))[HEAD_DIM:, :].astype(BF16)
+        vt[0:HEAD_DIM, 0:count] = jnp.transpose(block)[HEAD_DIM:, :]
 
     def score(c, block):
         return dot(block[:, 0:HEAD_DIM], q_all[:, c * CHUNK:(c + 1) * CHUNK])
@@ -261,11 +256,11 @@
         top[:, cut] = highest
 
     def attend(begin, stop, block, fresh, after=None):
-        ready = score(begin, block)
+        ready = [score(c, block) for c in range(begin, min(begin + DEPTH, stop))]
         for c in range(begin, stop):
-            now = ready
-            if c + 1 < stop:
-                ready = score(c + 1, block)
+            now = ready.pop(0)
+            if c + DEPTH < stop:
+                ready.append(score(c + DEPTH, block))
             absorb(c, now, fresh)
             if after is not None:
                 after(c)
@@ -274,11 +269,8 @@
     vt[HEAD_DIM:, :] = jnp.ones((vt.shape[0] - HEAD_DIM, vt.shape[1]), BF16)
     local_block = iota((8, LANES), 0)
     set_bias(jnp.where(local_block < blocks, kv * blocks + local_block, -2), blocks, True)
-    set_values(kv_all[tp])
-    own = kv_own[...]
-    attend(0, chunks, own, True)
-
-    def choose(flag, base):
+    set_values(kv_own[...])
+    def choose(flag):
         rank = jnp.zeros((1, LANES), F32)
         weight = [[], []]
         label = [jnp.zeros((1, LANES), F32) for _ in range(HOT)]
@@ -296,29 +288,25 @@
             total = total + block(b) * weight[b]
         return total
 
-    @pl.when(lead)
-    def _():
-        def name_take(i, total):
-            name_copy(i).wait_recv()
-            return total + names_in[i]
-
-        total = lax.fori_loop(0, after_far, name_take, jnp.zeros(names.shape[1:], F32))
-        total = jnp.where(total > 0.5, 1.0, 0.0)
-        weight, label = choose([total[b:b + 1, :] for b in range(blocks)], 0)
-        for s in range(HOT):
-            ids[s:s + 1, :] = label[s]
-            for t in range(2):
+    def choose_from(flags):
+        return choose([flags[b:b + 1, :] for b in range(blocks)])
+
+    def hot_send(i, _):
+        name_copy(i).wait_recv()
+        weight, _ = choose_from(names_in[i])
+        for t in range(2):
+            for s in range(HOT):
                 part = gather(weight[s], lambda b: kv_all[t, b * BLOCK:(b + 1) * BLOCK, :])
-                pack[t, s * BLOCK:(s + 1) * BLOCK, :] = part.astype(BF16)
-
-        def hot_send(i, _):
-            for t in range(2):
-                ids_copy(i, t).start()
-            for t in range(2):
-                hot_copy(i, t).start()
-            return 0
-
-        lax.fori_loop(0, after_far, hot_send, 0)
+                pack[i, t, s * BLOCK:(s + 1) * BLOCK, :] = part.astype(BF16)
+            hot_copy(i, t).start()
+        return 0
+
+    ahead = kv % 2 == 1
+    lax.fori_loop(0, jnp.where(ahead, 0, hots_out), hot_send, 0)
+
+    own = kv_own[...]
+    attend(0, chunks, own, True)
+    lax.fori_loop(0, jnp.where(ahead, hots_out, 0), hot_send, 0)
 
     def near_wait(i, _):
         near_copy(i).wait_recv()
@@ -329,7 +317,7 @@
         found += [jnp.full((1, LANES), -2, jnp.int32)] * (8 - len(found))
         return jnp.concatenate(found, axis=0)
 
-    chosen = [choose([names[i, b:b + 1, :] for b in range(blocks)], 0) for i in range(near)]
+    chosen = [choose_from(names[i]) for i in range(near)]
     set_bias(key_blocks([((kv - 1 - i) * blocks, v) for i in range(near) for v in chosen[i][1]]), near * HOT, False)
     lax.fori_loop(0, before_near, near_wait, 0)
     for i in range(near):
@@ -346,20 +334,18 @@
             src_ref=att.at[h], dst_ref=att_in.at[h], send_sem=att_s.at[h], recv_sem=att_r.at[h],
             device_id={"tp": 1 - tp}, device_id_type=MESH)
 
-    def ids_wait(i, _):
-        ids_copy(i, tp).wait_recv()
-        return 0
-
     def hot_wait(i, _):
         hot_copy(i, tp).wait_recv()
         return 0
 
-    lax.fori_loop(0, before_far, ids_wait, 0)
     width = att.shape[2]
     halves = att.shape[0]
 
     def far_bias(start):
-        labels = [((kv - 1 - near - start - i) * blocks, ids_in[start + i, s:s + 1, :]) for i in range(STEP) for s in range(HOT)]
+        labels = []
+        for i in range(STEP):
+            _, label = choose_from(names[near + start + i])
+            labels += [((kv - 1 - near - start - i) * blocks, v) for v in label]
         set_bias(key_blocks(labels), STEP * HOT, False)
 
     def far_block(start):
@@ -393,16 +379,16 @@
 
             def scaled(t):
                 cut = slice((p * per + t) * LANES, (p * per + t + 1) * LANES)
-                return acc[0:HEAD_DIM, cut] * (1.0 / acc[HEAD_DIM:HEAD_DIM + 1, cut])
+                return (acc[0:HEAD_DIM, cut] * (1.0 / acc[HEAD_DIM:HEAD_DIM + 1, cut])).astype(BF16)
 
             for m in range(main):
                 part = jnp.transpose(jnp.concatenate([scaled(2 * m), scaled(2 * m + 1)], axis=0))
-                att[h, m * LANES:(m + 1) * LANES, at:at + LANES] = part.astype(BF16)
+                att[h, m * LANES:(m + 1) * LANES, at:at + LANES] = part
             if tail:
                 part = scaled(per - 1)
                 turned = jnp.transpose(jnp.concatenate([part, part], axis=0))
                 part = jnp.where(low_tile, turned[0:SPAN], turned[SPAN:])
-                att[h, main * LANES:, at:at + LANES] = part.astype(BF16)
+                att[h, main * LANES:, at:at + LANES] = part
         att_copy(h).start()
 
     attend(0, chunks, block, False, finish)
@@ -440,7 +426,6 @@
 
     def hot_done(i, _):
         for t in range(2):
-            ids_copy(i, t).wait_send()
             hot_copy(i, t).wait_send()
         return 0
 
@@ -491,10 +476,8 @@
                 pltpu.VMEM((rows, LANES), BF16),
                 pltpu.VMEM((near, rows, LANES), BF16),
                 pltpu.VMEM((near * payload, LANES), BF16),
-                pltpu.VMEM((2, payload, LANES), BF16),
+                pltpu.VMEM((far, 2, payload, LANES), BF16),
                 pltpu.VMEM((far, payload, LANES), BF16),
-                pltpu.VMEM((HOT, LANES), F32),
-                pltpu.VMEM((far, HOT, LANES), F32),
                 pltpu.VMEM((most, -(-rows // LANES) * LANES), F32),
                 pltpu.VMEM((HEAD_DIM + 16, most), BF16),
                 pltpu.VMEM((HEAD_DIM, heads * rows), BF16),
@@ -504,7 +487,7 @@
                 pltpu.VMEM((2, rows, width), BF16),
                 pltpu.VMEM((rows, columns), F32),
                 dma((10,)), dma((far,)), dma((far,)), dma((near,)), dma((near,)),
-                dma((far, 2)), dma((far,)), dma((far, 2)), dma((far,)), dma((2,)), dma((2,)),
+                dma((far, 2)), dma((far,)), dma((2,)), dma((2,)),
             ],
             compiler_params=pltpu.CompilerParams(
                 collective_id=0, has_side_effects=True, vmem_limit_bytes=28 * 1024 * 1024

time: 11.8 us -> 11.4 us (0.966)
  Pallas kernels: 10.7 us -> 10.4 us
    pallas_call x1, Pallas kernels: 10.7 us -> 10.4 us  [shards(): pl.pallas_call(functools.partial(kernel, n, near, far), out_shape=jax.Sha...]
where the time goes in v3:
time: 11.4 us; the launch traced here: 11.3 us
  Pallas kernels  10.4 us (91%)
  local copies, waits for them, and re-layouts  0.88 us (8%)
    pallas_call x1, Pallas kernels, shards(): pl.pallas_call(functools.partial(kernel, n, near, far), out_shape=jax.Sha...  10.4 us
    unnamed x1, local copies, waits for them, and re-layouts  0.88 us

profile of v3, /device:TPU:25, one launch (start us, length us, event | category | flops | bytes accessed | tf_op | source)
XLA Modules:
  0.0 11.3 jit_solution(3137434875668804787)
XLA Ops:
  0.0 10.4 %shard_map.91 = bf16[1,192,2048]{2,1,0:T(8,128)(2,1)S(1)} custom-call(bf16[1,192,2048]{2,1,0:T(8,128)(2,1)} %tok_hbm.1, s32[1,8]{1,0:T(1,128)} %doc_hbm.1, s32[6,1,32]{2,1,0:T(1,128)} %bitcast.1, bf16[2048,512]{1,0:T(8,128)(2,1)} %wq_hbm.1, bf16[2048,128]{1,0:T(8,128)(2,1)} %wk_hbm.1, bf16[2048,128]{1,0:T(8,128)(2,1)} %wv_hbm.1, bf16[1024,2048]{1,0:T(8,128)(2,1)} %wo_hbm.1, ...), custom_call_target="tpu_custom_call" | custom-call | tf_op jit(solution)/shard_map/pallas_call | solution.py:459
  10.4 0.9 %copy.11 = bf16[1,192,2048]{2,1,0:T(8,128)(2,1)} copy(bf16[1,192,2048]{2,1,0:T(8,128)(2,1)S(1)} %shard_map.91) | data formatting | bytes 1572864

commit v4 on v3

--- a/solution.py
+++ b/solution.py
@@ -17,6 +17,7 @@
 NEAR = 2
 STEP = 2
 CHUNK = 256
+PIECES = 4
 DEPTH = 6
 MESH = pl.DeviceIdType.MESH
 SCALE = float(HEAD_DIM ** -0.5 * np.log2(np.e))
@@ -56,9 +57,9 @@
 
 
 def kernel(
-    n, near, far, tok_hbm, doc_hbm, pick_hbm, wq_hbm, wk_hbm, wv_hbm, wo_hbm, inner_hbm, outer_hbm, out,
+    n, near, far, tok_hbm, doc_hbm, pick_hbm, wq_hbm, wk_hbm, wv_hbm, wo_hbm, inner_hbm, outer_hbm, partial, last, w_last,
     tok, doc, pick, wq, wkv, wo, inner, outer, names, names_in, kv_all, kv_own, near_in, near_keys, pack, hot_in,
-    bias, vt, q_all, acc, top, att, att_in, partial,
+    bias, vt, q_all, acc, top, att, att_in,
     load_sem, name_s, name_r, near_s, near_r, hot_s, hot_r, att_s, att_r,
 ):
     kv = lax.axis_index("kv")
@@ -66,7 +67,9 @@
     rows = tok.shape[0]
     blocks = rows // BLOCK
     heads = wq.shape[1] // HEAD_DIM
-    mine = wo.shape[1]
+    width = att.shape[2]
+    halves = att.shape[0]
+    mine = halves * width
     pad = names.shape[1]
     kept = HOT * BLOCK
     lead = tp == 1
@@ -95,12 +98,14 @@
     pairs = [
         (pick_hbm, pick), (tok_hbm.at[0], tok), (wk_hbm, wkv.at[:, 0:LANES]), (wv_hbm, wkv.at[:, LANES:]),
         (inner_hbm, inner), (outer_hbm.at[kv], outer), (doc_hbm, doc), (wq_hbm, wq),
-        (wo_hbm.at[pl.ds(tp * mine, mine)], wo.at[0]), (wo_hbm.at[pl.ds((1 - tp) * mine, mine)], wo.at[1]),
+        (wo_hbm.at[pl.ds(tp * mine, mine)], wo.at[0:mine]),
+        (wo_hbm.at[pl.ds((1 - tp) * mine, mine - width)], wo.at[mine:]),
+        (wo_hbm.at[pl.ds((1 - tp) * mine + mine - width, width)], w_last),
     ]
     loads = [pltpu.make_async_copy(a, b, load_sem.at[i]) for i, (a, b) in enumerate(pairs)]
     for load in loads:
         load.start()
-    l_pick, l_tok, l_wk, l_wv, l_in, l_out, l_doc, l_wq, l_wo0, l_wo1 = loads
+    l_pick, l_tok, l_wk, l_wv, l_in, l_out, l_doc, l_wq, l_wo0, l_wo1, l_wo2 = loads
 
     def clear_near(i, _):
         near_in[i] = jnp.zeros(near_in.shape[1:], BF16)
@@ -306,7 +311,7 @@
 
     own = kv_own[...]
     attend(0, chunks, own, True)
-    lax.fori_loop(0, jnp.where(ahead, hots_out, 0), hot_send, 0)
+    lax.fori_loop(0, jnp.where(ahead, jnp.minimum(hots_out, 1), 0), hot_send, 0)
 
     def near_wait(i, _):
         near_copy(i).wait_recv()
@@ -329,6 +334,8 @@
     set_values(block)
     attend(0, chunks, block, False)
 
+    lax.fori_loop(1, jnp.where(ahead, hots_out, 1), hot_send, 0)
+
     def att_copy(h):
         return pltpu.make_async_remote_copy(
             src_ref=att.at[h], dst_ref=att_in.at[h], send_sem=att_s.at[h], recv_sem=att_r.at[h],
@@ -338,8 +345,6 @@
         hot_copy(i, tp).wait_recv()
         return 0
 
-    width = att.shape[2]
-    halves = att.shape[0]
 
     def far_bias(start):
         labels = []
@@ -394,13 +399,13 @@
     attend(0, chunks, block, False, finish)
 
     l_wo0.wait()
-    columns = wo.shape[2]
+    columns = wo.shape[1]
     piece = columns // 4
     for c in range(4):
         cut = slice(c * piece, (c + 1) * piece)
-        value = dot(att[0], wo[0, 0:width, cut])
+        value = dot(att[0], wo[0:width, cut])
         for h in range(1, halves):
-            value += dot(att[h], wo[0, h * width:(h + 1) * width, cut])
+            value += dot(att[h], wo[h * width:(h + 1) * width, cut])
         partial[:, cut] = value
     l_wo1.wait()
     att_copy(0).wait_recv()
@@ -409,12 +414,10 @@
             att_copy(h).wait_recv()
         for c in range(4):
             cut = slice(c * piece, (c + 1) * piece)
-            partial[:, cut] += dot(att_in[h], wo[1, h * width:(h + 1) * width, cut])
+            partial[:, cut] += dot(att_in[h], wo[mine + h * width:mine + (h + 1) * width, cut])
     att_copy(halves - 1).wait_recv()
-    for c in range(4):
-        cut = slice(c * piece, (c + 1) * piece)
-        value = partial[:, cut] + dot(att_in[halves - 1], wo[1, (halves - 1) * width:halves * width, cut])
-        out[0, :, cut] = value.astype(BF16)
+    last[...] = att_in[halves - 1]
+    l_wo2.wait()
 
     def name_done(i, _):
         name_copy(i).wait_send()
@@ -434,6 +437,19 @@
     lax.fori_loop(0, hots_out, hot_done, 0)
     for h in range(halves):
         att_copy(h).wait_send()
+
+
+def finish(partial, last, weight, out, stage, sem):
+    wide = stage.shape[2]
+    stores = []
+    for c in range(stage.shape[0]):
+        cut = slice(c * wide, (c + 1) * wide)
+        stage[c] = (partial[:, cut] + dot(last[...], weight[:, cut])).astype(BF16)
+        store = pltpu.make_async_copy(stage.at[c], out.at[0, :, cut], sem.at[c])
+        store.start()
+        stores.append(store)
+    for store in stores:
+        store.wait()
 
 
 def solution(mesh):
@@ -456,18 +472,23 @@
         most = max(rows, near * payload, STEP * payload)
         operands = (tokens, doc_lengths, jnp.transpose(picked, (1, 0, 2)), w_query, w_key, w_value, w_out, inner, outer)
         operands = [pltpu.with_memory_space_constraint(jnp.asarray(x), pltpu.HBM) for x in operands]
-        return pl.pallas_call(
+        vmem = pl.BlockSpec(memory_space=pltpu.VMEM)
+        parts = pl.pallas_call(
             functools.partial(kernel, n, near, far),
-            out_shape=jax.ShapeDtypeStruct((1, rows, columns), BF16),
+            out_shape=[
+                jax.ShapeDtypeStruct((rows, columns), F32),
+                jax.ShapeDtypeStruct((rows, width), BF16),
+                jax.ShapeDtypeStruct((width, columns), BF16),
+            ],
             in_specs=[pl.BlockSpec(memory_space=pltpu.HBM)] * 9,
-            out_specs=pl.BlockSpec(memory_space=pltpu.VMEM),
+            out_specs=[vmem] * 3,
             scratch_shapes=[
                 pltpu.VMEM((rows, d), BF16),
                 pltpu.SMEM(doc_lengths.shape, jnp.int32),
                 pltpu.VMEM((blocks, 1, picked.shape[2]), jnp.int32),
                 pltpu.VMEM(w_query.shape, BF16),
                 pltpu.VMEM((d, 2 * LANES), BF16),
-                pltpu.VMEM((2, w_out.shape[0] // 2, columns), BF16),
+                pltpu.VMEM((w_out.shape[0] - width, columns), BF16),
                 pltpu.VMEM(inner.shape, F32),
                 pltpu.VMEM(outer.shape[1:], F32),
                 pltpu.VMEM((near + far, pad, LANES), F32),
@@ -485,14 +506,21 @@
                 pltpu.VMEM((1, heads * rows), F32),
                 pltpu.VMEM((2, rows, width), BF16),
                 pltpu.VMEM((2, rows, width), BF16),
-                pltpu.VMEM((rows, columns), F32),
-                dma((10,)), dma((far,)), dma((far,)), dma((near,)), dma((near,)),
+                dma((11,)), dma((far,)), dma((far,)), dma((near,)), dma((near,)),
                 dma((far, 2)), dma((far,)), dma((2,)), dma((2,)),
             ],
             compiler_params=pltpu.CompilerParams(
                 collective_id=0, has_side_effects=True, vmem_limit_bytes=28 * 1024 * 1024
             ),
         )(*operands)
+        return pl.pallas_call(
+            finish,
+            out_shape=jax.ShapeDtypeStruct((1, rows, columns), BF16),
+            in_specs=[vmem] * 3,
+            out_specs=pl.BlockSpec(memory_space=pltpu.HBM),
+            scratch_shapes=[pltpu.VMEM((PIECES, rows, columns // PIECES), BF16), dma((PIECES,))],
+            compiler_params=pltpu.CompilerParams(vmem_limit_bytes=8 * 1024 * 1024),
+        )(*parts)
 
     placed = (P("dp", "kv", None), P("dp", None), P("dp", "kv", None), P(None, "tp"), P(), P(), P())
     return jax.shard_map(

time: 11.4 us -> 11 us (0.965)
  local copies, waits for them, and re-layouts: 0.88 us -> 0 us
  Pallas kernels: 10.4 us -> 10.8 us
    unnamed x1 -> x0, local copies, waits for them, and re-layouts: 0.88 us -> none
    pallas_call x1 -> x2, Pallas kernels: 10.4 us -> 10.8 us  [the longest x1 9.7 us: shards(): pl.pallas_call(functools.partial(kernel, n, near, far), out_shape=[jax.Sh...]
where the time goes in v4:
time: 11 us; the launch traced here: 10.9 us
  Pallas kernels  10.8 us (98%)
    pallas_call x1, Pallas kernels, shards(): pl.pallas_call(functools.partial(kernel, n, near, far), out_shape=[jax.Sh...  9.7 us
    pallas_call x1, Pallas kernels, shards(): pl.pallas_call(finish, out_shape=jax.ShapeDtypeStruct((1, rows, columns),...  1.15 us

profile of v4, /device:TPU:25, one launch (start us, length us, event | category | flops | bytes accessed | tf_op | source)
XLA Modules:
  0.0 10.9 jit_solution(15278018557694289691)
XLA Ops:
  0.0 9.7 %shard_map.91 = (f32[192,2048]{1,0:T(8,128)S(1)}, bf16[192,256]{1,0:T(8,128)(2,1)S(1)}, bf16[256,2048]{1,0:T(8,128)(2,1)S(1)}) custom-call(bf16[1,192,2048]{2,1,0:T(8,128)(2,1)} %tok_hbm.1, s32[1,8]{1,0:T(1,128)} %doc_hbm.1, s32[6,1,32]{2,1,0:T(1,128)} %bitcast.1, bf16[2048,512]{1,0:T(8,128)(2,1)} %wq_hbm.1, bf16[2048,128]{1,0:T(8,128)(2,1)} %wk_hbm.1, ...), custom_call_target="tpu_custom_call" | custom-call | tf_op jit(solution)/shard_map/pallas_call | solution.py:476
  9.7 1.1 %shard_map.92 = bf16[1,192,2048]{2,1,0:T(8,128)(2,1)} custom-call(f32[192,2048]{1,0:T(8,128)S(1)} %get-tuple-element.8.partial, bf16[192,256]{1,0:T(8,128)(2,1)S(1)} %get-tuple-element.9.last, bf16[256,2048]{1,0:T(8,128)(2,1)S(1)} %get-tuple-element.10.weight), custom_call_target="tpu_custom_call" | custom-call | tf_op jit(solution)/shard_map/pallas_call | solution.py:516

commit v5 on v4

--- a/solution.py
+++ b/solution.py
@@ -375,10 +375,7 @@
     block = far_block((steps - 1) * STEP)
     low_tile = iota((SPAN, LANES), 1) < HEAD_DIM
 
-    def finish(c):
-        if (c + 1) * halves % chunks:
-            return
-        h = (c + 1) * halves // chunks - 1
+    def finish_half(h):
         for p in range(h * heads // 2 // halves, (h + 1) * heads // 2 // halves):
             at = p * LANES - h * width
 
@@ -396,7 +393,15 @@
                 att[h, main * LANES:, at:at + LANES] = part
         att_copy(h).start()
 
-    attend(0, chunks, block, False, finish)
+    some = chunks // halves
+    ready = [score(c, block) for c in range(some)]
+    for h in range(halves):
+        now = ready
+        for c in range(some):
+            absorb(h * some + c, now[c], False)
+        if h + 1 < halves:
+            ready = [score((h + 1) * some + c, block) for c in range(some)]
+        finish_half(h)
 
     l_wo0.wait()
     columns = wo.shape[1]
@@ -440,14 +445,16 @@
 
 
 def finish(partial, last, weight, out, stage, sem):
+    pieces = stage.shape[0]
     wide = stage.shape[2]
-    stores = []
-    for c in range(stage.shape[0]):
-        cut = slice(c * wide, (c + 1) * wide)
-        stage[c] = (partial[:, cut] + dot(last[...], weight[:, cut])).astype(BF16)
-        store = pltpu.make_async_copy(stage.at[c], out.at[0, :, cut], sem.at[c])
-        store.start()
-        stores.append(store)
+    cuts = [slice(c * wide, (c + 1) * wide) for c in range(pieces)]
+    stores = [pltpu.make_async_copy(stage.at[c], out.at[0, :, cuts[c]], sem.at[c]) for c in range(pieces)]
+    ready = dot(last[...], weight[:, cuts[0]])
+    for c in range(pieces):
+        stage[c] = (partial[:, cuts[c]] + ready).astype(BF16)
+        if c + 1 < pieces:
+            ready = dot(last[...], weight[:, cuts[c + 1]])
+        stores[c].start()
     for store in stores:
         store.wait()
 

time: 11 us -> 11 us (level)
  no operation moved by 1% of the time
where the time goes in v5:
time: 11 us; the launch traced here: 10.8 us
  Pallas kernels  10.8 us (98%)
    pallas_call x1, Pallas kernels, shards(): pl.pallas_call(functools.partial(kernel, n, near, far), out_shape=[jax.Sh...  9.7 us
    pallas_call x1, Pallas kernels, shards(): pl.pallas_call(finish, out_shape=jax.ShapeDtypeStruct((1, rows, columns),...  1.14 us

profile of v5, /device:TPU:25, one launch (start us, length us, event | category | flops | bytes accessed | tf_op | source)
XLA Modules:
  0.0 10.8 jit_solution(12010659349488462840)
XLA Ops:
  0.0 9.7 %shard_map.91 = (f32[192,2048]{1,0:T(8,128)S(1)}, bf16[192,256]{1,0:T(8,128)(2,1)S(1)}, bf16[256,2048]{1,0:T(8,128)(2,1)S(1)}) custom-call(bf16[1,192,2048]{2,1,0:T(8,128)(2,1)} %tok_hbm.1, s32[1,8]{1,0:T(1,128)} %doc_hbm.1, s32[6,1,32]{2,1,0:T(1,128)} %bitcast.1, bf16[2048,512]{1,0:T(8,128)(2,1)} %wq_hbm.1, bf16[2048,128]{1,0:T(8,128)(2,1)} %wk_hbm.1, ...), custom_call_target="tpu_custom_call" | custom-call | tf_op jit(solution)/shard_map/pallas_call | solution.py:483
  9.7 1.1 %shard_map.92 = bf16[1,192,2048]{2,1,0:T(8,128)(2,1)} custom-call(f32[192,2048]{1,0:T(8,128)S(1)} %get-tuple-element.8.partial, bf16[192,256]{1,0:T(8,128)(2,1)S(1)} %get-tuple-element.9.last, bf16[256,2048]{1,0:T(8,128)(2,1)S(1)} %get-tuple-element.10.weight), custom_call_target="tpu_custom_call" | custom-call | tf_op jit(solution)/shard_map/pallas_call | solution.py:523
